TPU v7x, 32 devices: a whole 2x2x4 slice. The times are simulated.
32 devices in a mesh: fs: 16 (over z, y, x), tp: 2 (over core).
Axes of the slice: x: 2, y: 2, z: 4, core: 2. Of those that a mesh axis runs over, the one named last changes fastest.
Arguments:
- tokens: bfloat16 [4096, 2048], P('fs', 'tp'), may hold values from -6 to 6
- mixer_norm_gain: bfloat16 [2048], replicated, may hold values from 0.099609375 to 1.8984375
- recurrence_branch_weight: bfloat16 [2048, 1024], P('fs', 'tp'), may hold values from -0.125 to 0.125
- output_gate_projection: bfloat16 [2048, 1024], P('fs', 'tp'), may hold values from -0.125 to 0.125
- recurrence_conv_taps: bfloat16 [4, 1024], P(None, 'tp'), may hold values from -3 to 3
- recurrence_gate_map: bfloat16 [16, 64, 64], P('tp'), may hold values from -0.75 to 0.75
- input_gate_map: bfloat16 [16, 64, 64], P('tp'), may hold values from -0.75 to 0.75
- channel_decay_rate: float32 [1024], P('tp'), may hold values from 0.001 to 0.03
- position_log_decay: float32 [4096, 1024], P('fs', 'tp'), may hold values from -0.69 to 0
- mixer_output_weight: bfloat16 [1024, 2048], P('tp', 'fs'), may hold values from -0.75 to 0.75
- feedforward_norm_gain: bfloat16 [2048], replicated, may hold values from 0.099609375 to 1.8984375
- gate_up_weight: bfloat16 [2048, 5632], P('fs', 'tp'), may hold values from -0.125 to 0.125
- value_up_weight: bfloat16 [2048, 5632], P('fs', 'tp'), may hold values from -0.125 to 0.125
- gate_conv_taps: bfloat16 [3, 5632], P(None, 'tp'), may hold values from -3 to 3
- value_conv_taps: bfloat16 [3, 5632], P(None, 'tp'), may hold values from -3 to 3
- down_projection_weight: bfloat16 [5632, 2048], P('tp', 'fs'), may hold values from -0.15625 to 0.15625
Outputs:
- result: bfloat16 [4096, 2048], P('fs', 'tp')
All inputs are finite; a program needn't handle non-finite values.
Results may differ from a plain program's by a relative error of at most 0.024.
Values may be sent and summed in bfloat16 or wider, within the bound.
A program may use at most 128 MiB of HBM per device.

v0:
```python
import jax
import jax.numpy as jnp
from jax import lax
from jax.sharding import PartitionSpec as P

SEQ_LEN = 64


EPS = 1e-06
DECAY_RATE_GAIN = 8.0


def rms_normed(values, gain):
    wide = values.astype(jnp.float32)
    factor = lax.rsqrt(jnp.mean(wide * wide, axis=-1, keepdims=True) + EPS)
    return (wide * factor * gain.astype(jnp.float32)).astype(jnp.bfloat16)


def causal_conv(values, kernel):
    width = kernel.shape[0]
    row_count, channels = values.shape
    grouped = values.astype(jnp.float32).reshape(row_count // SEQ_LEN, SEQ_LEN, channels)
    padded = jnp.pad(grouped, ((0, 0), (width - 1, 0), (0, 0)))
    summed = padded[:, 0:SEQ_LEN] * kernel[0].astype(jnp.float32)
    for offset in range(1, width):
        summed = summed + padded[:, offset : offset + SEQ_LEN] * kernel[offset].astype(jnp.float32)
    return summed.reshape(row_count, channels)


def combine(left, right):
    first_a, first_b = left
    second_a, second_b = right
    return (first_a * second_a, second_a * first_b + second_b)


def pair_folder(normed, pieces):
    return (
        jnp.dot(normed, pieces[0], preferred_element_type=jnp.float32),
        jnp.dot(normed, pieces[1], preferred_element_type=jnp.float32),
    )


def per_device(
    tokens,
    mixer_norm_gain,
    recurrence_branch_weight,
    output_gate_projection,
    recurrence_conv_taps,
    recurrence_gate_map,
    input_gate_map,
    channel_decay_rate,
    position_log_decay,
    mixer_output_weight,
    feedforward_norm_gain,
    gate_up_weight,
    value_up_weight,
    gate_conv_taps,
    value_conv_taps,
    down_projection_weight,
):
    row_count = tokens.shape[0]
    local_width = recurrence_branch_weight.shape[1]
    local_heads = recurrence_gate_map.shape[0]
    head_size = recurrence_gate_map.shape[1]
    whole_rows = lax.all_gather(tokens, "tp", axis=1, tiled=True)
    normed = rms_normed(whole_rows, mixer_norm_gain)
    branch_sum, outgate_sum = pair_folder(
        normed,
        (
            lax.all_gather(recurrence_branch_weight, "fs", axis=0, tiled=True),
            lax.all_gather(output_gate_projection, "fs", axis=0, tiled=True),
        ),
    )
    branch = branch_sum.astype(jnp.bfloat16)
    outgate = outgate_sum.astype(jnp.bfloat16)
    conv = causal_conv(branch, recurrence_conv_taps).astype(jnp.bfloat16)
    grouped = conv.reshape(row_count, local_heads, head_size)
    recurrence_scan = jax.nn.sigmoid(
        jnp.einsum(
            "rhi,hij->rhj", grouped, recurrence_gate_map, preferred_element_type=jnp.float32
        ).reshape(row_count, local_width)
    )
    inner = jax.nn.sigmoid(
        jnp.einsum(
            "rhi,hij->rhj", grouped, input_gate_map, preferred_element_type=jnp.float32
        ).reshape(row_count, local_width)
    )
    log_alpha = (
        -DECAY_RATE_GAIN * recurrence_scan * channel_decay_rate[None, :] + position_log_decay
    )
    drive = jnp.sqrt(-jnp.expm1(2.0 * log_alpha)) * inner * conv.astype(jnp.float32)
    shape3 = (row_count // SEQ_LEN, SEQ_LEN, local_width)
    unused, state = lax.associative_scan(
        combine, (jnp.exp(log_alpha).reshape(shape3), drive.reshape(shape3)), axis=1
    )
    state = state.reshape(row_count, local_width)
    mixed = (state * jax.nn.gelu(outgate.astype(jnp.float32))).astype(jnp.bfloat16)
    mixer_terms = jnp.dot(
        mixed,
        lax.all_gather(mixer_output_weight, "fs", axis=1, tiled=True),
        preferred_element_type=jnp.float32,
    )
    mixer_terms = mixer_terms.astype(jnp.bfloat16).astype(jnp.float32)
    mixer_whole = lax.psum(mixer_terms.astype(jnp.bfloat16), "tp").astype(jnp.float32)
    whole_after = (whole_rows.astype(jnp.float32) + mixer_whole).astype(jnp.bfloat16)
    normed2 = rms_normed(whole_after, feedforward_norm_gain)
    gate_whole, value_whole = (
        lax.all_gather(gate_up_weight, "fs", axis=0, tiled=True),
        lax.all_gather(value_up_weight, "fs", axis=0, tiled=True),
    )
    gate_sum = jnp.dot(normed2, gate_whole, preferred_element_type=jnp.float32)
    value_sum = jnp.dot(normed2, value_whole, preferred_element_type=jnp.float32)
    gate_half = gate_sum.astype(jnp.bfloat16)
    value_half = value_sum.astype(jnp.bfloat16)
    hidden = (
        jax.nn.silu(causal_conv(gate_half, gate_conv_taps))
        * causal_conv(value_half, value_conv_taps)
    ).astype(jnp.bfloat16)
    channel_terms = jnp.dot(
        hidden,
        lax.all_gather(down_projection_weight, "fs", axis=1, tiled=True),
        preferred_element_type=jnp.float32,
    )
    channel_terms = channel_terms.astype(jnp.bfloat16).astype(jnp.float32)
    channel_share = lax.psum_scatter(
        channel_terms.astype(jnp.bfloat16), "tp", scatter_dimension=1, tiled=True
    ).astype(jnp.float32)
    share_width = channel_share.shape[1]
    residual_share = lax.dynamic_slice_in_dim(
        whole_after, lax.axis_index("tp") * share_width, share_width, 1
    )
    return (residual_share.astype(jnp.float32) + channel_share).astype(jnp.bfloat16)


def solution(mesh):
    placed = (
        P("fs", "tp"),
        P(),
        P("fs", "tp"),
        P("fs", "tp"),
        P(None, "tp"),
        P("tp", None, None),
        P("tp", None, None),
        P("tp"),
        P("fs", "tp"),
        P("tp", "fs"),
        P(),
        P("fs", "tp"),
        P("fs", "tp"),
        P(None, "tp"),
        P(None, "tp"),
        P("tp", "fs"),
    )
    return jax.shard_map(
        per_device, mesh=mesh, in_specs=placed, out_specs=P("fs", "tp"), check_vma=False
    )
```

profile of v0, /device:TPU:10, one launch (start us, length us, event | category | flops | bytes accessed | tf_op | source)
XLA Modules:
  0.0 726.9 jit_solution(12462820517022480084)
XLA Ops:
  6.5 0.7 all-gather.8.cloned.1.call-update
  7.3 0.0 all-gather.10.cloned.1.call-start
  7.3 0.7 all-gather.10.cloned.1.call-update
  8.0 0.0 all-gather.12.cloned.1.call-start
  8.1 0.7 all-gather.12.cloned.1.call-update
  8.8 0.5 all-gather.14.cloned.1.call-update
  9.3 0.0 all-reduce.17.cloned.1.call-start
  9.4 0.7 convert_element_type.188
  10.1 0.8 slice_convert_fusion.3
  10.9 0.7 broadcast_multiply_fusion
  11.6 7.8 %all-gather.8.cloned.1.call-done = bf16[256,2048]{1,0:T(8,128)(2,1)} async-done(((bf16[256,1024]{1,0:T(8,128)(2,1)}), bf16[256,2048]{1,0:T(8,128)(2,1)}) %all-gather.8.cloned.1.call-update) | async-done | bytes 1048592 | tf_op jit(solution)/shard_map/all_gather | solution.py:65
  19.3 1.5 fusion.15
  20.9 62.3 %all-gather.10.cloned.1.call-done = bf16[2048,512]{1,0:T(8,128)(2,1)} async-done(((bf16[128,512]{1,0:T(8,128)(2,1)}), bf16[2048,512]{1,0:T(8,128)(2,1)}) %all-gather.10.cloned.1.call-update) | async-done | bytes 2097168 | tf_op jit(solution)/shard_map/all_gather | solution.py:70
  83.2 2.7 convolution_convert_fusion.5
  85.9 0.1 convert.14
  86.0 0.2 fusion.30
  86.2 0.3 convert_element_type.200
  86.5 0.3 copy.22
  86.8 0.4 fusion.22
  87.2 0.2 copy.24
  87.4 0.4 fusion.24
  87.8 0.2 copy.27
  88.0 0.4 fusion.52
  88.4 0.1 slice.199
  88.6 0.1 slice.200
  88.7 0.1 slice.198
  88.9 0.1 slice.202
  89.0 0.1 fusion.64
  90.0 0.1 slice.203
  90.0 0.1 slice.236
  90.1 0.2 slice.238
  90.3 0.2 slice.197
  90.6 0.1 pad.52
  90.7 0.1 pad.51
  91.2 0.1 pad.57
  91.3 0.1 pad.58
  91.4 0.1 pad.60
  91.6 0.1 fusion.47
  91.7 0.1 pad.59
  91.8 0.1 add.183
  91.9 53.3 %all-gather.12.cloned.1.call-done = bf16[2048,512]{1,0:T(8,128)(2,1)} async-done(((bf16[128,512]{1,0:T(8,128)(2,1)}), bf16[2048,512]{1,0:T(8,128)(2,1)}) %all-gather.12.cloned.1.call-update) | async-done | bytes 2097168 | tf_op jit(solution)/shard_map/all_gather | solution.py:71
  145.2 61.9 %all-gather.14.cloned.1.call-done = bf16[512,2048]{1,0:T(8,128)(2,1)} async-done(((bf16[512,128]{1,0:T(8,128)(2,1)}), bf16[512,2048]{1,0:T(8,128)(2,1)}) %all-gather.14.cloned.1.call-update) | async-done | bytes 2097168 | tf_op jit(solution)/shard_map/all_gather | solution.py:100
  207.1 4.7 convolution_convert_fusion.3
  211.8 0.0 all-gather.18.cloned.1.call-start
  211.9 0.5 all-gather.18.cloned.1.call-update
  212.4 0.7 all-gather.16.cloned.1.call-update
  213.2 0.7 all-gather.20.cloned.1.call-update
  213.9 0.2 reduce-scatter.2.cloned.1.call-start
  214.1 0.1 convert_reduce_fusion.2
  214.3 0.1 convert_reduce_fusion.5
  214.4 18.2 %all-reduce.17.cloned.1.call-done = bf16[256,2048]{1,0:T(8,128)(2,1)} async-done(((bf16[256,2048]{1,0:T(8,128)(2,1)}), bf16[256,2048]{1,0:T(8,128)(2,1)}) %all-reduce.17.cloned.1.call-update) | async-done | bytes 1048592 | tf_op jit(solution)/shard_map/psum | solution.py:104
  232.5 1.7 fusion.12
  234.3 141.4 %all-gather.18.cloned.1.call-done = bf16[2048,2816]{1,0:T(8,128)(2,1)} async-done(((bf16[128,2816]{1,0:T(8,128)(2,1)}), bf16[2048,2816]{1,0:T(8,128)(2,1)}) %all-gather.18.cloned.1.call-update) | async-done | bytes 11534352 | tf_op jit(solution)/shard_map/all_gather | solution.py:109
  375.7 7.5 %convolution_convert_fusion = bf16[256,2816]{1,0:T(8,128)(2,1)S(1)} fusion(bf16[2048,2816]{1,0:T(8,128)(2,1)} %all-gather.18.cloned.1.call-done, bf16[256,2048]{1,0:T(8,128)(2,1)S(1)} %get-tuple-element.12, f32[2048]{0:T(1024)S(1)} %convert_element_type.211, f32[256]{0:T(256)S(1)} %add_rsqrt_fusion), kind=kOutput, calls=%fused_computation | convolution fusion | flops 2955608064 | bytes 14033920 | tf_op jit(solution)/shard_map/dot_general | solution.py:112
  383.2 0.2 convert.16
  383.4 134.7 %all-gather.16.cloned.1.call-done = bf16[2048,2816]{1,0:T(8,128)(2,1)} async-done(((bf16[128,2816]{1,0:T(8,128)(2,1)}), bf16[2048,2816]{1,0:T(8,128)(2,1)}) %all-gather.16.cloned.1.call-update) | async-done | bytes 11534352 | tf_op jit(solution)/shard_map/all_gather | solution.py:108
  518.1 7.8 %convolution_convert_fusion.1 = bf16[256,2816]{1,0:T(8,128)(2,1)S(1)} fusion(bf16[2048,2816]{1,0:T(8,128)(2,1)} %all-gather.16.cloned.1.call-done, bf16[256,2048]{1,0:T(8,128)(2,1)} %copy-done.3, f32[2048]{0:T(1024)S(1)} %convert_element_type.211, f32[256]{0:T(256)S(1)} %add_rsqrt_fusion), kind=kOutput, calls=%fused_computation.1 | convolution fusion | flops 2955608064 | bytes 14033920 | tf_op jit(solution)/shard_map/dot_general | solution.py:111
  525.9 0.2 convert.15
  526.1 1.8 fusion.2
  527.9 0.8 fusion.8
  528.8 171.3 %all-gather.20.cloned.1.call-done = bf16[2816,2048]{1,0:T(8,128)(2,1)} async-done(((bf16[2816,128]{1,0:T(8,128)(2,1)}), bf16[2816,2048]{1,0:T(8,128)(2,1)}) %all-gather.20.cloned.1.call-update) | async-done | bytes 11534352 | tf_op jit(solution)/shard_map/all_gather | solution.py:121
  700.1 8.5 %convolution_convert_fusion.2 = bf16[256,2048]{1,0:T(8,128)(2,1)} fusion(bf16[256,2816]{1,0:T(8,128)(2,1)S(1)} %fusion.8, bf16[2816,2048]{1,0:T(8,128)(2,1)} %all-gather.20.cloned.1.call-done), kind=kOutput, calls=%fused_computation.26 | convolution fusion | flops 2953314304 | bytes 14024704 | tf_op jit(solution)/shard_map/dot_general | solution.py:119
  708.6 9.8 %reduce-scatter.2.cloned.1.call-done = bf16[256,1024]{1,0:T(8,128)(2,1)} async-done(((bf16[256,2048]{1,0:T(8,128)(2,1)}), bf16[256,1024]{1,0:T(8,128)(2,1)}) %reduce-scatter.2.cloned.1.call-update) | async-done | bytes 524304 | tf_op jit(solution)/shard_map/reduce_scatter | solution.py:125
  718.3 2.0 add_convert_fusion
  (76 shorter events, 1.5 us)
Async XLA Ops:
  6.5 80.3 %copy-start = (bf16[8,64,64]{2,1,0:T(8,128)(2,1)S(1)}, bf16[8,64,64]{2,1,0:T(8,128)(2,1)}, u32[]{:S(2)}) copy-start(bf16[8,64,64]{2,1,0:T(8,128)(2,1)} %param.21) | copy-start | bytes 196612
  6.5 12.8 %all-gather.8.cloned.1.call-start = ((), (), s32[]{:S(2)}) async-start(), calls=%async_computation.1 | async-start | bytes 1572864 | tf_op jit(solution)/shard_map/all_gather | solution.py:65
  7.3 75.9 %all-gather.10.cloned.1.call-start = ((), (), s32[]{:S(2)}) async-start(), calls=%async_computation.2 | async-start | bytes 2228224 | tf_op jit(solution)/shard_map/all_gather | solution.py:70
  8.0 137.2 %all-gather.12.cloned.1.call-start = ((), (), s32[]{:S(2)}) async-start(), calls=%async_computation.3 | async-start | bytes 2228224 | tf_op jit(solution)/shard_map/all_gather | solution.py:71
  8.7 198.3 %all-gather.14.cloned.1.call-start = ((), (), s32[]{:S(2)}) async-start(), calls=%async_computation.4 | async-start | bytes 2228224 | tf_op jit(solution)/shard_map/all_gather | solution.py:100
  9.3 223.2 %all-reduce.17.cloned.1.call-start = ((), (), s32[]{:S(2)}) async-start(), calls=%async_computation.5 | async-start | bytes 2097152 | tf_op jit(solution)/shard_map/psum | solution.py:104
  86.0 1.5 copy-start.9
  86.8 1.2 copy-start.5
  91.4 115.7 %copy-start.2 = (bf16[256,2048]{1,0:T(8,128)(2,1)S(1)}, bf16[256,2048]{1,0:T(8,128)(2,1)}, u32[]{:S(2)}) copy-start(bf16[256,2048]{1,0:T(8,128)(2,1)} %all-gather.8.cloned.1.call-done) | copy-start | bytes 3145732
  211.8 2.3 copy-start.8
  211.8 2.4 copy-start.6
  211.8 2.5 copy-start.7
  211.8 163.9 %all-gather.18.cloned.1.call-start = ((), (), s32[]{:S(2)}) async-start(), calls=%async_computation.7 | async-start | bytes 12255232 | tf_op jit(solution)/shard_map/all_gather | solution.py:109
  212.4 305.7 %all-gather.16.cloned.1.call-start = ((), (), s32[]{:S(2)}) async-start(), calls=%async_computation.6 | async-start | bytes 12255232 | tf_op jit(solution)/shard_map/all_gather | solution.py:108
  213.1 486.9 %all-gather.20.cloned.1.call-start = ((), (), s32[]{:S(2)}) async-start(), calls=%async_computation.8 | async-start | bytes 12255232 | tf_op jit(solution)/shard_map/all_gather | solution.py:121
  213.9 504.4 %reduce-scatter.2.cloned.1.call-start = ((), (), s32[]{:S(2)}) async-start(), calls=%async_computation.9 | async-start | bytes 1572864 | tf_op jit(solution)/shard_map/reduce_scatter | solution.py:125
  234.3 148.9 %copy-start.3 = (bf16[256,2048]{1,0:T(8,128)(2,1)}, bf16[256,2048]{1,0:T(8,128)(2,1)S(1)}, u32[]{:S(2)}) copy-start(bf16[256,2048]{1,0:T(8,128)(2,1)S(1)} %get-tuple-element.12) | copy-start | bytes 3145732
  528.8 189.6 %copy-start.4 = (bf16[256,2048]{1,0:T(8,128)(2,1)S(1)}, bf16[256,2048]{1,0:T(8,128)(2,1)}, u32[]{:S(2)}) copy-start(bf16[256,2048]{1,0:T(8,128)(2,1)} %copy-done.3) | copy-start | bytes 3145732
  700.1 20.3 %copy-start.1 = (bf16[8,64,64]{2,1,0:T(8,128)(2,1)S(1)}, bf16[8,64,64]{2,1,0:T(8,128)(2,1)}, u32[]{:S(2)}) copy-start(bf16[8,64,64]{2,1,0:T(8,128)(2,1)} %param.21) | copy-start | bytes 196612
Sparse Core Ops, SparseCore 0:
  8.9 10.4 all-gather.7
  22.1 61.0 all-gather.9
  86.0 59.1 all-gather.11
  147.7 59.2 all-gather.13
  211.9 20.5 all-reduce.16
  235.1 140.5 all-gather.17
  378.5 139.5 all-gather.15
  520.8 179.2 all-gather.19
  708.7 9.5 reduce-scatter.1
where the time goes:
time: 729 us; the launch traced here: 727 us
  waiting for transfers between devices  665 us (91%)
  matrix products  31.8 us (4%)
  between operations  13.8 us (2%)
  other arithmetic  12.2 us (2%)
    all_gather x1, waiting for transfers between devices, per_device(): lax.all_gather(down_projection_weight, 'fs', axis=1, tiled=True)  171 us
    all_gather x1, waiting for transfers between devices, per_device(): lax.all_gather(value_up_weight, 'fs', axis=0, tiled=True)  141 us
    all_gather x1, waiting for transfers between devices, per_device(): lax.all_gather(gate_up_weight, 'fs', axis=0, tiled=True)  135 us
    all_gather x1, waiting for transfers between devices, per_device(): lax.all_gather(recurrence_branch_weight, 'fs', axis=0, tiled=True)  62.3 us
    all_gather x1, waiting for transfers between devices, per_device(): lax.all_gather(mixer_output_weight, 'fs', axis=1, tiled=True)  61.9 us
    all_gather x1, waiting for transfers between devices, per_device(): lax.all_gather(output_gate_projection, 'fs', axis=0, tiled=True)  53.3 us
    psum x1, waiting for transfers between devices, per_device(): lax.psum(mixer_terms.astype(jnp.bfloat16), 'tp').astype(jnp.float32)  18.2 us
  transfers between devices with their start and end apart: 9, of which 9 were waited for; matrix products, arithmetic and copies ran while one was open for 4% of the time, Pallas kernels for 0%

commit v1 on v0

--- a/solution.py
+++ b/solution.py
@@ -1,6 +1,10 @@
+import functools
+
 import jax
 import jax.numpy as jnp
 from jax import lax
+from jax.experimental import pallas as pl
+from jax.experimental.pallas import tpu as pltpu
 from jax.sharding import PartitionSpec as P
 
 SEQ_LEN = 64
@@ -40,7 +44,7 @@
     )
 
 
-def per_device(
+def gathered_layer(
     tokens,
     mixer_norm_gain,
     recurrence_branch_weight,
@@ -132,6 +136,357 @@
     return (residual_share.astype(jnp.float32) + channel_share).astype(jnp.bfloat16)
 
 
+PLANE = 4
+ANY = pl.BlockSpec(memory_space=pl.ANY)
+
+
+def hop(src, dst, send, recv, target):
+    return pltpu.make_async_remote_copy(
+        src_ref=src,
+        dst_ref=dst,
+        send_sem=send,
+        recv_sem=recv,
+        device_id=target,
+        device_id_type=pl.DeviceIdType.MESH,
+    )
+
+
+def greet(targets):
+    barrier = pltpu.get_barrier_semaphore()
+    for target in targets:
+        pl.semaphore_signal(
+            barrier, inc=1, device_id=target, device_id_type=pl.DeviceIdType.MESH
+        )
+    pl.semaphore_wait(barrier, len(targets))
+
+
+def span(index, size):
+    return pl.ds(pl.multiple_of(index * size, size), size)
+
+
+def where_am_i(layers):
+    fs, tp = lax.axis_index("fs"), lax.axis_index("tp")
+    return fs, fs // PLANE, fs % PLANE, tp
+
+
+def line_targets(layers, z, p, tp):
+    return [(((z + s) % layers) * PLANE + p, tp) for s in range(1, layers)]
+
+
+def weights_kernel(
+    layers, tok, bo, mo, gu, dn, whole_tok, bo_all, mo_all, gu_all, dn_all, send, recv, tok_sems, local
+):
+    fs, z, p, tp = where_am_i(layers)
+    y, x = p // 2, p % 2
+    px, py = y * 2 + (x + 1) % 2, ((y + 1) % 2) * 2 + x
+    pd = ((y + 1) % 2) * 2 + (x + 1) % 2
+    x_target, y_target = (z * PLANE + px, tp), (z * PLANE + py, tp)
+    core_target = (fs, 1 - tp)
+    on_line = line_targets(layers, z, p, tp)
+    greet(on_line + [x_target, y_target, core_target])
+
+    half = tok.shape[1]
+    deep = bo.shape[0]
+    wide = mo.shape[1]
+
+    def bo_at(f, part=None):
+        if part is None:
+            return bo_all.at[span(f, deep), :]
+        return bo_all.at[span(f * 2 + part, deep // 2), :]
+
+    def gu_at(f, part=None):
+        if part is None:
+            return gu_all.at[span(f, deep), :]
+        return gu_all.at[span(f * 2 + part, deep // 2), :]
+
+    def mo_at(f, part=None):
+        rows = mo.shape[0]
+        if part is None:
+            return mo_all.at[:, span(f, wide)]
+        return mo_all.at[pl.ds(part * (rows // 2), rows // 2), span(f, wide)]
+
+    def dn_at(f, part=None):
+        rows = dn.shape[1]
+        if part is None:
+            return dn_all.at[:, span(f, wide)]
+        return dn_all.at[pl.ds(part * (rows // 2), rows // 2), span(f, wide)]
+
+    arrays = (
+        (bo_at, lambda zz: bo),
+        (mo_at, lambda zz: mo),
+        (gu_at, lambda zz: gu.at[zz]),
+        (dn_at, lambda zz: dn.at[zz]),
+    )
+    tok_copy = hop(tok, whole_tok.at[:, span(tp, half)], tok_sems.at[0], tok_sems.at[1], core_target)
+    tok_copy.start()
+    own = [pltpu.make_async_copy(tok, whole_tok.at[:, span(tp, half)], local.at[len(arrays)])]
+    for a, (at, source) in enumerate(arrays):
+        own.append(pltpu.make_async_copy(source(z), at(fs), local.at[a]))
+    for copy in own:
+        copy.start()
+
+    line = {}
+    for a, (at, source) in enumerate(arrays):
+        for s in range(1, layers):
+            line[a, s] = hop(
+                source((z + s) % layers), at(fs), send.at[a, 0, s], recv.at[a, 0, s], on_line[s - 1]
+            )
+            line[a, s].start()
+
+    sides, corners = {}, {}
+
+    def start_sides(a, s):
+        at, source = arrays[a]
+        f = ((z - s + layers) % layers) * PLANE + p
+        block = source(z) if s == 0 else at(f)
+        for kind, target in ((1, x_target), (2, y_target)):
+            sides[a, kind, s] = hop(block, at(f), send.at[a, kind, s], recv.at[a, kind, s], target)
+            sides[a, kind, s].start()
+
+    def start_corners(a, s):
+        at, source = arrays[a]
+        base = ((z - s + layers) % layers) * PLANE
+        for kind, part, owner, target in ((1, 0, px, y_target), (2, 1, py, x_target)):
+            sides[a, kind, s].wait_recv()
+            block = at(base + owner, part)
+            copy = hop(block, block, send.at[a, kind + 2, s], recv.at[a, kind + 2, s], target)
+            copy.start()
+            corners[a, kind, s] = copy
+
+    steps = [(a, 0) for a in range(len(arrays))]
+    for first in (0, 2):
+        for s in range(1, layers):
+            for a in (first, first + 1):
+                steps.append((a, s))
+    order = [(0, 0), (1, 0)] + [q for q in steps if q[0] < 2 and q[1] > 0]
+    order += [(2, 0), (3, 0)] + [q for q in steps if q[0] > 1 and q[1] > 0]
+    lag = 2
+    for i in range(len(order) + lag):
+        if i < len(order):
+            a, s = order[i]
+            if s > 0:
+                line[a, s].wait_recv()
+            start_sides(a, s)
+        if i >= lag:
+            start_corners(*order[i - lag])
+
+    for a, s in order:
+        if s > 0:
+            line[a, s].wait_send()
+        for kind in (1, 2):
+            sides[a, kind, s].wait_send()
+            corners[a, kind, s].wait()
+    for copy in own:
+        copy.wait()
+    tok_copy.wait()
+
+
+def gather_weights(layers, tok, bo, mo, gu, dn):
+    n_fs = layers * PLANE
+    shape = jax.ShapeDtypeStruct
+    kind = jnp.bfloat16
+    return pl.pallas_call(
+        functools.partial(weights_kernel, layers),
+        out_shape=(
+            shape((tok.shape[0], 2 * tok.shape[1]), kind),
+            shape((n_fs * bo.shape[0], bo.shape[1]), kind),
+            shape((mo.shape[0], n_fs * mo.shape[1]), kind),
+            shape((n_fs * gu.shape[1], gu.shape[2]), kind),
+            shape((dn.shape[1], n_fs * dn.shape[2]), kind),
+        ),
+        in_specs=[ANY] * 5,
+        out_specs=(ANY,) * 5,
+        scratch_shapes=[
+            pltpu.SemaphoreType.DMA((4, 5, layers)),
+            pltpu.SemaphoreType.DMA((4, 5, layers)),
+            pltpu.SemaphoreType.DMA((2,)),
+            pltpu.SemaphoreType.DMA((5,)),
+        ],
+        compiler_params=pltpu.CompilerParams(collective_id=0, has_side_effects=True),
+        name="gather_weights",
+    )(tok, bo, mo, gu, dn)
+
+
+def swap_kernel(mine, theirs, sems):
+    target = (lax.axis_index("fs"), 1 - lax.axis_index("tp"))
+    greet([target])
+    copy = hop(mine, theirs, sems.at[0], sems.at[1], target)
+    copy.start()
+    copy.wait()
+
+
+def swap_cores(values, number):
+    return pl.pallas_call(
+        swap_kernel,
+        out_shape=jax.ShapeDtypeStruct(values.shape, values.dtype),
+        in_specs=[ANY],
+        out_specs=ANY,
+        scratch_shapes=[pltpu.SemaphoreType.DMA((2,))],
+        compiler_params=pltpu.CompilerParams(collective_id=number, has_side_effects=True),
+        name="swap_cores",
+    )(values)
+
+
+def rows_kernel(layers, mine, whole, send, recv, local):
+    fs, z, p, tp = where_am_i(layers)
+    core_target = (fs, 1 - tp)
+    on_line = line_targets(layers, z, p, tp)
+    greet(on_line + [core_target])
+    rows, half = mine.shape[0], mine.shape[1] // 2
+    own = pltpu.make_async_copy(mine, whole.at[span(z, rows), :], local.at[0])
+    line = {}
+    for s in range(1, layers):
+        line[s] = hop(
+            mine.at[:, span(tp, half)],
+            whole.at[span(z, rows), span(tp, half)],
+            send.at[0, s],
+            recv.at[0, s],
+            on_line[s - 1],
+        )
+        line[s].start()
+    own.start()
+    across = {}
+    for s in range(1, layers):
+        line[s].wait_recv()
+        block = whole.at[span((z - s + layers) % layers, rows), span(tp, half)]
+        across[s] = hop(block, block, send.at[1, s], recv.at[1, s], core_target)
+        across[s].start()
+    for s in range(1, layers):
+        line[s].wait_send()
+        across[s].wait()
+    own.wait()
+
+
+def gather_rows(layers, values):
+    return pl.pallas_call(
+        functools.partial(rows_kernel, layers),
+        out_shape=jax.ShapeDtypeStruct((layers * values.shape[0], values.shape[1]), values.dtype),
+        in_specs=[ANY],
+        out_specs=ANY,
+        scratch_shapes=[
+            pltpu.SemaphoreType.DMA((2, layers)),
+            pltpu.SemaphoreType.DMA((2, layers)),
+            pltpu.SemaphoreType.DMA((1,)),
+        ],
+        compiler_params=pltpu.CompilerParams(collective_id=2, has_side_effects=True),
+        name="gather_rows",
+    )(values)
+
+
+def deal_kernel(layers, mine, dealt, send, recv):
+    fs, z, p, tp = where_am_i(layers)
+    on_line = line_targets(layers, z, p, tp)
+    greet(on_line)
+    line = {}
+    for s in range(1, layers):
+        line[s] = hop(
+            mine.at[(z + s) % layers], dealt.at[s - 1], send.at[s], recv.at[s], on_line[s - 1]
+        )
+        line[s].start()
+    for s in range(1, layers):
+        line[s].wait()
+
+
+def deal_rows(layers, values):
+    return pl.pallas_call(
+        functools.partial(deal_kernel, layers),
+        out_shape=jax.ShapeDtypeStruct((layers - 1,) + values.shape[1:], values.dtype),
+        in_specs=[ANY],
+        out_specs=ANY,
+        scratch_shapes=[
+            pltpu.SemaphoreType.DMA((layers,)),
+            pltpu.SemaphoreType.DMA((layers,)),
+        ],
+        compiler_params=pltpu.CompilerParams(collective_id=3, has_side_effects=True),
+        name="deal_rows",
+    )(values)
+
+
+def split_layer(
+    layers,
+    tokens,
+    mixer_norm_gain,
+    recurrence_branch_weight,
+    output_gate_projection,
+    recurrence_conv_taps,
+    recurrence_gate_map,
+    input_gate_map,
+    channel_decay_rate,
+    position_log_decay,
+    mixer_output_weight,
+    feedforward_norm_gain,
+    gate_up_weight,
+    value_up_weight,
+    gate_conv_taps,
+    value_conv_taps,
+    down_projection_weight,
+):
+    row_count, half = tokens.shape
+    local_width = recurrence_branch_weight.shape[1]
+    local_heads, head_size = recurrence_gate_map.shape[:2]
+    deep, local_units = gate_up_weight.shape
+    units = local_units // layers
+    z, tp = lax.axis_index("fs") // PLANE, lax.axis_index("tp")
+    bo = jnp.concatenate([recurrence_branch_weight, output_gate_projection], axis=1)
+    gu = jnp.concatenate(
+        [
+            gate_up_weight.reshape(deep, layers, units),
+            value_up_weight.reshape(deep, layers, units),
+        ],
+        axis=2,
+    ).transpose(1, 0, 2)
+    dn = down_projection_weight.reshape(layers, units, down_projection_weight.shape[1])
+    whole_rows, bo_all, mo_all, gu_all, dn_all = gather_weights(
+        layers, tokens, bo, mixer_output_weight, gu, dn
+    )
+    normed = rms_normed(whole_rows, mixer_norm_gain)
+    both = jnp.dot(normed, bo_all, preferred_element_type=jnp.float32).astype(jnp.bfloat16)
+    branch, outgate = both[:, :local_width], both[:, local_width:]
+    conv = causal_conv(branch, recurrence_conv_taps).astype(jnp.bfloat16)
+    grouped = conv.reshape(row_count, local_heads, head_size)
+
+    def gate_of(weight):
+        return jax.nn.sigmoid(
+            jnp.einsum(
+                "rhi,hij->rhj", grouped, weight, preferred_element_type=jnp.float32
+            ).reshape(row_count, local_width)
+        )
+
+    recur, inner = gate_of(recurrence_gate_map), gate_of(input_gate_map)
+    log_alpha = -DECAY_RATE_GAIN * recur * channel_decay_rate[None, :] + position_log_decay
+    drive = jnp.sqrt(-jnp.expm1(2.0 * log_alpha)) * inner * conv.astype(jnp.float32)
+    shape3 = (row_count // SEQ_LEN, SEQ_LEN, local_width)
+    unused, state = lax.associative_scan(
+        combine, (jnp.exp(log_alpha).reshape(shape3), drive.reshape(shape3)), axis=1
+    )
+    state = state.reshape(row_count, local_width)
+    mixed = (state * jax.nn.gelu(outgate.astype(jnp.float32))).astype(jnp.bfloat16)
+    mine = jnp.dot(mixed, mo_all, preferred_element_type=jnp.float32).astype(jnp.bfloat16)
+    theirs = swap_cores(mine, 1)
+    mixer_whole = mine.astype(jnp.float32) + theirs.astype(jnp.float32)
+    whole_after = (whole_rows.astype(jnp.float32) + mixer_whole).astype(jnp.bfloat16)
+    normed2 = gather_rows(layers, rms_normed(whole_after, feedforward_norm_gain))
+    halves = jnp.dot(normed2, gu_all, preferred_element_type=jnp.float32).astype(jnp.bfloat16)
+    gate_taps = lax.dynamic_slice_in_dim(gate_conv_taps, z * units, units, 1)
+    value_taps = lax.dynamic_slice_in_dim(value_conv_taps, z * units, units, 1)
+    hidden = (
+        jax.nn.silu(causal_conv(halves[:, :units], gate_taps))
+        * causal_conv(halves[:, units:], value_taps)
+    ).astype(jnp.bfloat16)
+    share = jnp.dot(hidden, dn_all, preferred_element_type=jnp.float32).astype(jnp.bfloat16)
+    kept = lax.dynamic_slice_in_dim(share, tp * half, half, 1)
+    given = lax.dynamic_slice_in_dim(share, (1 - tp) * half, half, 1)
+    from_core = swap_cores(given, 4)
+    paired = (kept.astype(jnp.float32) + from_core.astype(jnp.float32)).astype(jnp.bfloat16)
+    paired = paired.reshape(layers, row_count, half)
+    dealt = deal_rows(layers, paired)
+    total = lax.dynamic_index_in_dim(paired, z, 0, keepdims=False).astype(jnp.float32)
+    for s in range(layers - 1):
+        total = total + dealt[s].astype(jnp.float32)
+    residual = lax.dynamic_slice_in_dim(whole_after, tp * half, half, 1)
+    return (residual.astype(jnp.float32) + total).astype(jnp.bfloat16)
+
+
 def solution(mesh):
     placed = (
         P("fs", "tp"),
@@ -151,6 +506,11 @@
         P(None, "tp"),
         P("tp", "fs"),
     )
+    n_fs, n_tp = mesh.shape["fs"], mesh.shape["tp"]
+    layers = n_fs // PLANE
+    body = gathered_layer
+    if n_tp == 2 and n_fs % PLANE == 0 and layers > 1:
+        body = functools.partial(split_layer, layers)
     return jax.shard_map(
-        per_device, mesh=mesh, in_specs=placed, out_specs=P("fs", "tp"), check_vma=False
-    )
+        body, mesh=mesh, in_specs=placed, out_specs=P("fs", "tp"), check_vma=False
+    )

time: 729 us -> 311 us (0.43)
  waiting for transfers between devices: 665 us -> 0 us
  Pallas kernels: 0 us -> 252 us
  between operations: 13.8 us -> 0.8 us
  local copies, waits for them, and re-layouts: 3.45 us -> 13.4 us
  matrix products: 31.8 us -> 23 us
  other arithmetic: 12.2 us -> 20.7 us
    all_gather x7 -> x0, waiting for transfers between devices: 633 us -> none  [the longest x1 171 us: per_device(): lax.all_gather(down_projection_weight, 'fs', axis=1, tiled=True)]
    pallas_call x0 -> x5, Pallas kernels: none -> 252 us  [the longest x1 138 us: gather_weights(): pl.pallas_call(functools.partial(weights_kernel, layers), out_shape=(shap...]
    psum x1 -> x0, waiting for transfers between devices: 18.2 us -> none  [per_device(): lax.psum(mixer_terms.astype(jnp.bfloat16), 'tp').astype(jnp.float32)]
    reduce_scatter x1 -> x0, waiting for transfers between devices: 9.75 us -> none  [per_device(): lax.psum_scatter(channel_terms.astype(jnp.bfloat16), 'tp', scatter_dimens...]
    dot_general x7 -> x6, matrix products: 31.8 us -> 23 us  [the longest x1 10.1 us: split_layer(): jnp.dot(normed2, gu_all, preferred_element_type=jnp.float32)]
  transfers between devices with their start and end apart: 9 -> 0, of which waited for: 9 -> 0; matrix products, arithmetic and copies ran while one was open for 4% -> 0% of each run, Pallas kernels for 0% -> 0%
where the time goes in v1:
time: 311 us; the launch traced here: 310 us
  Pallas kernels  252 us (81%)
  matrix products  23 us (7%)
  other arithmetic  20.7 us (7%)
  local copies, waits for them, and re-layouts  13.4 us (4%)
    pallas_call x1, Pallas kernels, gather_weights(): pl.pallas_call(functools.partial(weights_kernel, layers), out_shape=(shap...  138 us
    pallas_call x1, Pallas kernels, gather_rows(): pl.pallas_call(functools.partial(rows_kernel, layers), out_shape=jax.Shap...  58 us
    pallas_call x1, Pallas kernels, deal_rows(): pl.pallas_call(functools.partial(deal_kernel, layers), out_shape=jax.Shap...  49 us
    dot_general x1, matrix products, split_layer(): jnp.dot(normed2, gu_all, preferred_element_type=jnp.float32)  10.1 us
    pallas_call x2, Pallas kernels, swap_cores(): pl.pallas_call(swap_kernel, out_shape=jax.ShapeDtypeStruct(values.shape,...  7.54 us

profile of v1, /device:TPU:10, one launch (start us, length us, event | category | flops | bytes accessed | tf_op | source)
XLA Modules:
  0.0 310.2 jit_solution(3636282862304839748)
XLA Ops:
  0.0 1.5 copy.22
  1.5 0.3 copy.24
  1.8 0.0 copy-start.8
  1.9 0.0 copy-start.9
  1.9 0.3 copy.23
  2.2 0.3 copy.25
  2.5 0.0 copy-start.11
  2.5 1.6 maximum_bitcast_fusion.gu
  4.1 0.7 pad_maximum_fusion.bo
  4.8 137.8 %gather_weights.1 = (bf16[256,2048]{1,0:T(8,128)(2,1)}, bf16[2048,1024]{1,0:T(8,128)(2,1)}, bf16[512,2048]{1,0:T(8,128)(2,1)}, bf16[2048,1408]{1,0:T(8,128)(2,1)}, bf16[704,2048]{1,0:T(8,128)(2,1)}) custom-call(bf16[256,1024]{1,0:T(8,128)(2,1)} %tok.1, bf16[128,1024]{1,0:T(8,128)(2,1)} %pad_maximum_fusion.bo, bf16[512,128]{1,0:T(8,128)(2,1)} %mo.1, ...), custom_call_target="tpu_custom_call" | custom-call | tf_op jit(solution)/shard_map/gather_weights/pallas_call | solution.py:288
  142.6 1.5 fusion.15
  144.2 0.0 copy-start.10
  144.2 3.8 %convolution_convert_fusion.3 = bf16[256,1024]{1,0:T(8,128)(2,1)S(1)} fusion(bf16[2048,1024]{1,0:T(8,128)(2,1)} %get-tuple-element.11, bf16[256,2048]{1,0:T(8,128)(2,1)} %get-tuple-element.10, f32[2048]{0:T(1024)S(1)} %convert_element_type.203, f32[256]{0:T(256)S(1)} %add_rsqrt_fusion.1), kind=kOutput, calls=%fused_computation.36 | convolution fusion | flops 1076101120 | bytes 5776384 | tf_op jit(solution)/shard_map/dot_general | solution.py:443
  148.0 0.0 copy-start.15
  148.0 0.1 convert.14
  148.1 0.2 fusion.33
  148.4 0.3 convert_element_type.215
  148.7 0.3 copy.26
  149.0 0.0 copy-start.13
  149.0 0.4 fusion.22
  149.4 0.2 copy.28
  149.6 0.4 fusion.24
  150.0 0.2 copy.31
  150.2 0.4 fusion.44
  150.6 0.3 slice.221
  151.0 0.1 slice.222
  151.1 0.1 slice.220
  151.3 0.1 slice.224
  151.4 0.1 fusion.59
  152.3 0.1 pad.52
  152.4 0.1 pad.51
  153.0 0.1 slice.225
  153.0 0.1 slice.258
  153.2 0.1 pad.57
  153.3 0.1 pad.58
  153.4 0.1 pad.60
  153.6 0.2 slice.260
  153.7 0.2 slice.219
  153.9 0.1 fusion.43
  154.1 0.1 pad.59
  154.2 0.1 add.212
  154.3 0.2 fusion.42
  154.5 3.4 %convolution_convert_fusion.2.mine = bf16[256,2048]{1,0:T(8,128)(2,1)} fusion(bf16[256,512]{1,0:T(8,128)(2,1)S(1)} %fusion.42, bf16[512,2048]{1,0:T(8,128)(2,1)} %get-tuple-element.12), kind=kOutput, calls=%fused_computation.27 | convolution fusion | flops 537395200 | bytes 3407872 | tf_op jit(solution)/shard_map/dot_general | solution.py:464
  157.9 3.0 swap_cores.2
  160.9 2.2 fusion.12
  163.2 1.0 copy-done.2
  164.1 1.3 fusion.14.mine
  165.4 58.0 %gather_rows.1 = bf16[1024,2048]{1,0:T(8,128)(2,1)} custom-call(bf16[256,2048]{1,0:T(8,128)(2,1)} %fusion.14.mine), custom_call_target="tpu_custom_call" | custom-call | tf_op jit(solution)/shard_map/gather_rows/pallas_call | solution.py:361
  223.5 10.1 %convolution_convert_fusion = bf16[1024,1408]{1,0:T(8,128)(2,1)S(1)} fusion(bf16[1024,2048]{1,0:T(8,128)(2,1)} %gather_rows.1, bf16[2048,1408]{1,0:T(8,128)(2,1)} %get-tuple-element.13), kind=kOutput, calls=%fused_computation.1 | convolution fusion | flops 5907021824 | bytes 12845056 | tf_op jit(solution)/shard_map/dot_general | solution.py:469
  233.6 1.9 fusion.58
  235.5 0.3 convert.15
  235.9 0.9 fusion.53
  236.8 0.9 fusion.2
  237.8 0.5 copy-done.4
  238.2 0.3 convert.16
  238.6 0.9 fusion.6
  239.5 0.9 fusion.8
  240.5 0.9 copy-done.14
  241.3 4.9 %convolution_convert_fusion.1 = bf16[1024,2048]{1,0:T(8,128)(2,1)} fusion(bf16[1024,704]{1,0:T(8,128)(2,1)S(1)} %fusion.8, bf16[704,2048]{1,0:T(8,128)(2,1)S(1)} %copy-done.14), kind=kOutput, calls=%fused_computation.2 | convolution fusion | flops 2954887168 | bytes 8519680 | tf_op jit(solution)/shard_map/dot_general | solution.py:476
  246.3 3.1 constant_dynamic-slice_fusion.mine
  249.4 4.5 %swap_cores.3 = bf16[1024,1024]{1,0:T(8,128)(2,1)} custom-call(bf16[1024,1024]{1,0:T(8,128)(2,1)} %constant_dynamic-slice_fusion.mine), custom_call_target="tpu_custom_call" | custom-call | tf_op jit(solution)/shard_map/swap_cores/pallas_call | solution.py:319
  253.9 4.5 %add_convert_fusion = bf16[1024,1024]{1,0:T(8,128)(2,1)} fusion(bf16[1024,1024]{1,0:T(8,128)(2,1)} %swap_cores.3, bf16[1024,2048]{1,0:T(8,128)(2,1)} %convolution_convert_fusion.1, s32[]{:T(128)S(6)} %select_n.20), kind=kLoop, calls=%fused_computation | loop fusion | flops 4194304 | bytes 6291460 | tf_op jit(solution)/shard_map/convert_element_type | solution.py:480
  258.4 49.0 %deal_rows.1 = bf16[3,256,1024]{2,1,0:T(8,128)(2,1)} custom-call(bf16[4,256,1024]{2,1,0:T(8,128)(2,1)} %bitcast.71), custom_call_target="tpu_custom_call" | custom-call | tf_op jit(solution)/shard_map/deal_rows/pallas_call | solution.py:391
  307.4 2.8 fusion.26
  (77 shorter events, 1.4 us)
Async XLA Ops:
  0.0 149.0 %copy-start = (bf16[8,64,64]{2,1,0:T(8,128)(2,1)S(1)}, bf16[8,64,64]{2,1,0:T(8,128)(2,1)}, u32[]{:S(2)}) copy-start(bf16[8,64,64]{2,1,0:T(8,128)(2,1)} %param.21) | copy-start | bytes 196612
  0.0 1.8 copy-start.6
  1.8 2.3 copy-start.8
  1.9 2.3 copy-start.9
  2.5 141.6 %copy-start.11 = (bf16[2048]{0:T(1024)(128)(2,1)S(1)}, bf16[2048]{0:T(1024)(128)(2,1)}, u32[]{:S(2)}) copy-start(bf16[2048]{0:T(1024)(128)(2,1)} %param.17) | copy-start | bytes 12292
  144.2 3.9 %copy-start.10 = (bf16[4,512]{1,0:T(4,128)(2,1)S(1)}, bf16[4,512]{1,0:T(4,128)(2,1)}, u32[]{:S(2)}) copy-start(bf16[4,512]{1,0:T(4,128)(2,1)} %param.20) | copy-start | bytes 12292
  148.0 1.6 copy-start.15
  149.0 1.2 copy-start.13
  149.0 1.2 copy-start.7
  154.3 6.7 %copy-start.5 = (bf16[256,2048]{1,0:T(8,128)(2,1)S(1)}, bf16[256,2048]{1,0:T(8,128)(2,1)}, u32[]{:S(2)}) copy-start(bf16[256,2048]{1,0:T(8,128)(2,1)} %get-tuple-element.10) | copy-start | bytes 3145732
  157.9 5.2 %copy-start.12 = (bf16[2048]{0:T(1024)(128)(2,1)S(1)}, bf16[2048]{0:T(1024)(128)(2,1)}, u32[]{:S(2)}) copy-start(bf16[2048]{0:T(1024)(128)(2,1)} %param.26) | copy-start | bytes 12292
  163.1 1.0 copy-start.2
  236.8 1.4 copy-start.4
  239.5 1.8 copy-start.14
  258.4 49.0 %copy-start.3 = (bf16[256,2048]{1,0:T(8,128)(2,1)S(1)}, bf16[256,2048]{1,0:T(8,128)(2,1)}, u32[]{:S(2)}) copy-start(bf16[256,2048]{1,0:T(8,128)(2,1)} %copy-done.2) | copy-start | bytes 3145732
  258.4 51.8 %copy-start.1 = (bf16[8,64,64]{2,1,0:T(8,128)(2,1)S(1)}, bf16[8,64,64]{2,1,0:T(8,128)(2,1)}, u32[]{:S(2)}) copy-start(bf16[8,64,64]{2,1,0:T(8,128)(2,1)} %param.21) | copy-start | bytes 196612

commit v2 on v1

--- a/solution.py
+++ b/solution.py
@@ -94,7 +94,7 @@
     )
     drive = jnp.sqrt(-jnp.expm1(2.0 * log_alpha)) * inner * conv.astype(jnp.float32)
     shape3 = (row_count // SEQ_LEN, SEQ_LEN, local_width)
-    unused, state = lax.associative_scan(
+    _, state = lax.associative_scan(
         combine, (jnp.exp(log_alpha).reshape(shape3), drive.reshape(shape3)), axis=1
     )
     state = state.reshape(row_count, local_width)
@@ -164,58 +164,99 @@
     return pl.ds(pl.multiple_of(index * size, size), size)
 
 
-def where_am_i(layers):
+def where_am_i():
     fs, tp = lax.axis_index("fs"), lax.axis_index("tp")
     return fs, fs // PLANE, fs % PLANE, tp
 
 
 def line_targets(layers, z, p, tp):
     return [(((z + s) % layers) * PLANE + p, tp) for s in range(1, layers)]
+
+
+def share_plane(layers, z, p, tp, arrays, order, send, recv, arrived):
+    y, x = p // 2, p % 2
+    px, py = y * 2 + (x + 1) % 2, ((y + 1) % 2) * 2 + x
+    x_target, y_target = (z * PLANE + px, tp), (z * PLANE + py, tp)
+    sides, corners = {}, {}
+
+    def start_sides(a, s):
+        at, source = arrays[a]
+        f = ((z - s + layers) % layers) * PLANE + p
+        block = source(z) if s == 0 else at(f)
+        for kind, target in ((1, x_target), (2, y_target)):
+            sides[a, kind, s] = hop(block, at(f), send.at[a, kind, s], recv.at[a, kind, s], target)
+            sides[a, kind, s].start()
+
+    def start_corners(a, s):
+        at, _ = arrays[a]
+        base = ((z - s + layers) % layers) * PLANE
+        for kind, part, owner, target in ((1, 0, px, y_target), (2, 1, py, x_target)):
+            sides[a, kind, s].wait_recv()
+            block = at(base + owner, part)
+            copy = hop(block, block, send.at[a, kind + 2, s], recv.at[a, kind + 2, s], target)
+            copy.start()
+            corners[a, kind, s] = copy
+
+    lag = 2
+    for i in range(len(order) + lag):
+        if i < len(order):
+            arrived(*order[i])
+            start_sides(*order[i])
+        if i >= lag:
+            start_corners(*order[i - lag])
+
+    def finish():
+        for copy in sides.values():
+            copy.wait_send()
+        for copy in corners.values():
+            copy.wait()
+
+    return finish
+
+
+def row_blocks(whole, deep):
+    def at(f, part=None):
+        if part is None:
+            return whole.at[span(f, deep), :]
+        return whole.at[span(f * 2 + part, deep // 2), :]
+
+    return at
+
+
+def column_blocks(whole, wide):
+    rows = whole.shape[0]
+
+    def at(f, part=None):
+        if part is None:
+            return whole.at[:, span(f, wide)]
+        return whole.at[pl.ds(part * (rows // 2), rows // 2), span(f, wide)]
+
+    return at
+
+
+def plane_targets(z, p, tp):
+    y, x = p // 2, p % 2
+    px, py = y * 2 + (x + 1) % 2, ((y + 1) % 2) * 2 + x
+    return [(z * PLANE + px, tp), (z * PLANE + py, tp)]
 
 
 def weights_kernel(
     layers, tok, bo, mo, gu, dn, whole_tok, bo_all, mo_all, gu_all, dn_all, send, recv, tok_sems, local
 ):
-    fs, z, p, tp = where_am_i(layers)
-    y, x = p // 2, p % 2
-    px, py = y * 2 + (x + 1) % 2, ((y + 1) % 2) * 2 + x
-    pd = ((y + 1) % 2) * 2 + (x + 1) % 2
-    x_target, y_target = (z * PLANE + px, tp), (z * PLANE + py, tp)
+    fs, z, p, tp = where_am_i()
     core_target = (fs, 1 - tp)
     on_line = line_targets(layers, z, p, tp)
-    greet(on_line + [x_target, y_target, core_target])
+    greet(on_line + plane_targets(z, p, tp) + [core_target])
 
     half = tok.shape[1]
     deep = bo.shape[0]
     wide = mo.shape[1]
 
-    def bo_at(f, part=None):
-        if part is None:
-            return bo_all.at[span(f, deep), :]
-        return bo_all.at[span(f * 2 + part, deep // 2), :]
-
-    def gu_at(f, part=None):
-        if part is None:
-            return gu_all.at[span(f, deep), :]
-        return gu_all.at[span(f * 2 + part, deep // 2), :]
-
-    def mo_at(f, part=None):
-        rows = mo.shape[0]
-        if part is None:
-            return mo_all.at[:, span(f, wide)]
-        return mo_all.at[pl.ds(part * (rows // 2), rows // 2), span(f, wide)]
-
-    def dn_at(f, part=None):
-        rows = dn.shape[1]
-        if part is None:
-            return dn_all.at[:, span(f, wide)]
-        return dn_all.at[pl.ds(part * (rows // 2), rows // 2), span(f, wide)]
-
     arrays = (
-        (bo_at, lambda zz: bo),
-        (mo_at, lambda zz: mo),
-        (gu_at, lambda zz: gu.at[zz]),
-        (dn_at, lambda zz: dn.at[zz]),
+        (row_blocks(bo_all, deep), lambda zz: bo),
+        (column_blocks(mo_all, wide), lambda zz: mo),
+        (row_blocks(gu_all, deep), lambda zz: gu.at[zz]),
+        (column_blocks(dn_all, wide), lambda zz: dn.at[zz]),
     )
     tok_copy = hop(tok, whole_tok.at[:, span(tp, half)], tok_sems.at[0], tok_sems.at[1], core_target)
     tok_copy.start()
@@ -233,49 +274,20 @@
             )
             line[a, s].start()
 
-    sides, corners = {}, {}
-
-    def start_sides(a, s):
-        at, source = arrays[a]
-        f = ((z - s + layers) % layers) * PLANE + p
-        block = source(z) if s == 0 else at(f)
-        for kind, target in ((1, x_target), (2, y_target)):
-            sides[a, kind, s] = hop(block, at(f), send.at[a, kind, s], recv.at[a, kind, s], target)
-            sides[a, kind, s].start()
-
-    def start_corners(a, s):
-        at, source = arrays[a]
-        base = ((z - s + layers) % layers) * PLANE
-        for kind, part, owner, target in ((1, 0, px, y_target), (2, 1, py, x_target)):
-            sides[a, kind, s].wait_recv()
-            block = at(base + owner, part)
-            copy = hop(block, block, send.at[a, kind + 2, s], recv.at[a, kind + 2, s], target)
-            copy.start()
-            corners[a, kind, s] = copy
-
-    steps = [(a, 0) for a in range(len(arrays))]
-    for first in (0, 2):
-        for s in range(1, layers):
-            for a in (first, first + 1):
-                steps.append((a, s))
-    order = [(0, 0), (1, 0)] + [q for q in steps if q[0] < 2 and q[1] > 0]
-    order += [(2, 0), (3, 0)] + [q for q in steps if q[0] > 1 and q[1] > 0]
-    lag = 2
-    for i in range(len(order) + lag):
-        if i < len(order):
-            a, s = order[i]
-            if s > 0:
-                line[a, s].wait_recv()
-            start_sides(a, s)
-        if i >= lag:
-            start_corners(*order[i - lag])
-
-    for a, s in order:
+    def arrived(a, s):
         if s > 0:
-            line[a, s].wait_send()
-        for kind in (1, 2):
-            sides[a, kind, s].wait_send()
-            corners[a, kind, s].wait()
+            line[a, s].wait_recv()
+
+    order = [(a, 0) for a in range(2)]
+    order += [(a, s) for s in range(1, layers) for a in range(2)]
+    order += [(2, s) for s in range(layers // 2)]
+    finish = share_plane(layers, z, p, tp, arrays, order, send, recv, arrived)
+    for a, s in line:
+        if (a, s) not in order:
+            line[a, s].wait_recv()
+    finish()
+    for copy in line.values():
+        copy.wait_send()
     for copy in own:
         copy.wait()
     tok_copy.wait()
@@ -327,78 +339,88 @@
     )(values)
 
 
-def rows_kernel(layers, mine, whole, send, recv, local):
-    fs, z, p, tp = where_am_i(layers)
+def rows_kernel(
+    layers, mine, gu_in, dn_in, whole, gu_all, dn_all, send, recv, plane_send, plane_recv, local
+):
+    fs, z, p, tp = where_am_i()
     core_target = (fs, 1 - tp)
     on_line = line_targets(layers, z, p, tp)
-    greet(on_line + [core_target])
+    greet(on_line + plane_targets(z, p, tp) + [core_target])
     rows, half = mine.shape[0], mine.shape[1] // 2
-    own = pltpu.make_async_copy(mine, whole.at[span(z, rows), :], local.at[0])
-    line = {}
+    own = pltpu.make_async_copy(mine, whole.at[pl.ds((layers - 1) * rows, rows), :], local.at[0])
+    line, across = {}, {}
     for s in range(1, layers):
         line[s] = hop(
             mine.at[:, span(tp, half)],
-            whole.at[span(z, rows), span(tp, half)],
+            whole.at[pl.ds((layers - 1 - s) * rows, rows), span(tp, half)],
             send.at[0, s],
             recv.at[0, s],
             on_line[s - 1],
         )
         line[s].start()
     own.start()
-    across = {}
+    n_fs = layers * PLANE
+    arrays = []
+    for at in (row_blocks(gu_all, gu_all.shape[0] // n_fs), column_blocks(dn_all, dn_all.shape[1] // n_fs)):
+        arrays.append((at, lambda zz, at=at: at(zz * PLANE + p)))
+    order = [(0, s) for s in range(layers // 2, layers)] + [(1, s) for s in range(layers)]
+    finish = share_plane(
+        layers, z, p, tp, arrays, order, plane_send, plane_recv, lambda a, s: None
+    )
     for s in range(1, layers):
         line[s].wait_recv()
-        block = whole.at[span((z - s + layers) % layers, rows), span(tp, half)]
+        block = whole.at[pl.ds((layers - 1 - s) * rows, rows), span(tp, half)]
         across[s] = hop(block, block, send.at[1, s], recv.at[1, s], core_target)
         across[s].start()
     for s in range(1, layers):
         line[s].wait_send()
         across[s].wait()
+    finish()
     own.wait()
 
 
-def gather_rows(layers, values):
+def gather_rows(layers, values, gu_all, dn_all):
+    whole = jax.ShapeDtypeStruct((layers * values.shape[0], values.shape[1]), values.dtype)
     return pl.pallas_call(
         functools.partial(rows_kernel, layers),
-        out_shape=jax.ShapeDtypeStruct((layers * values.shape[0], values.shape[1]), values.dtype),
-        in_specs=[ANY],
-        out_specs=ANY,
+        out_shape=(
+            whole,
+            jax.ShapeDtypeStruct(gu_all.shape, gu_all.dtype),
+            jax.ShapeDtypeStruct(dn_all.shape, dn_all.dtype),
+        ),
+        in_specs=[ANY] * 3,
+        out_specs=(ANY,) * 3,
+        input_output_aliases={1: 1, 2: 2},
         scratch_shapes=[
             pltpu.SemaphoreType.DMA((2, layers)),
             pltpu.SemaphoreType.DMA((2, layers)),
+            pltpu.SemaphoreType.DMA((2, 5, layers)),
+            pltpu.SemaphoreType.DMA((2, 5, layers)),
             pltpu.SemaphoreType.DMA((1,)),
         ],
         compiler_params=pltpu.CompilerParams(collective_id=2, has_side_effects=True),
         name="gather_rows",
-    )(values)
-
-
-def deal_kernel(layers, mine, dealt, send, recv):
-    fs, z, p, tp = where_am_i(layers)
-    on_line = line_targets(layers, z, p, tp)
-    greet(on_line)
-    line = {}
-    for s in range(1, layers):
-        line[s] = hop(
-            mine.at[(z + s) % layers], dealt.at[s - 1], send.at[s], recv.at[s], on_line[s - 1]
-        )
-        line[s].start()
-    for s in range(1, layers):
-        line[s].wait()
-
-
-def deal_rows(layers, values):
+    )(values, gu_all, dn_all)
+
+
+def swap_half_kernel(mine, theirs, sems):
+    tp = lax.axis_index("tp")
+    target = (lax.axis_index("fs"), 1 - tp)
+    greet([target])
+    copy = hop(mine.at[:, span(1 - tp, theirs.shape[1])], theirs, sems.at[0], sems.at[1], target)
+    copy.start()
+    copy.wait()
+
+
+def swap_halves(values, number):
     return pl.pallas_call(
-        functools.partial(deal_kernel, layers),
-        out_shape=jax.ShapeDtypeStruct((layers - 1,) + values.shape[1:], values.dtype),
+        swap_half_kernel,
+        out_shape=jax.ShapeDtypeStruct((values.shape[0], values.shape[1] // 2), values.dtype),
         in_specs=[ANY],
         out_specs=ANY,
-        scratch_shapes=[
-            pltpu.SemaphoreType.DMA((layers,)),
-            pltpu.SemaphoreType.DMA((layers,)),
-        ],
-        compiler_params=pltpu.CompilerParams(collective_id=3, has_side_effects=True),
-        name="deal_rows",
+        scratch_shapes=[pltpu.SemaphoreType.DMA((2,))],
+        compiler_params=pltpu.CompilerParams(collective_id=number, has_side_effects=True),
+        name="swap_halves",
     )(values)
 
 
@@ -456,7 +478,7 @@
     log_alpha = -DECAY_RATE_GAIN * recur * channel_decay_rate[None, :] + position_log_decay
     drive = jnp.sqrt(-jnp.expm1(2.0 * log_alpha)) * inner * conv.astype(jnp.float32)
     shape3 = (row_count // SEQ_LEN, SEQ_LEN, local_width)
-    unused, state = lax.associative_scan(
+    _, state = lax.associative_scan(
         combine, (jnp.exp(log_alpha).reshape(shape3), drive.reshape(shape3)), axis=1
     )
     state = state.reshape(row_count, local_width)
@@ -465,24 +487,47 @@
     theirs = swap_cores(mine, 1)
     mixer_whole = mine.astype(jnp.float32) + theirs.astype(jnp.float32)
     whole_after = (whole_rows.astype(jnp.float32) + mixer_whole).astype(jnp.bfloat16)
-    normed2 = gather_rows(layers, rms_normed(whole_after, feedforward_norm_gain))
-    halves = jnp.dot(normed2, gu_all, preferred_element_type=jnp.float32).astype(jnp.bfloat16)
+    normed2, gu_all, dn_all = gather_rows(
+        layers, rms_normed(whole_after, feedforward_norm_gain), gu_all, dn_all
+    )
     gate_taps = lax.dynamic_slice_in_dim(gate_conv_taps, z * units, units, 1)
     value_taps = lax.dynamic_slice_in_dim(value_conv_taps, z * units, units, 1)
-    hidden = (
-        jax.nn.silu(causal_conv(halves[:, :units], gate_taps))
-        * causal_conv(halves[:, units:], value_taps)
-    ).astype(jnp.bfloat16)
-    share = jnp.dot(hidden, dn_all, preferred_element_type=jnp.float32).astype(jnp.bfloat16)
-    kept = lax.dynamic_slice_in_dim(share, tp * half, half, 1)
-    given = lax.dynamic_slice_in_dim(share, (1 - tp) * half, half, 1)
-    from_core = swap_cores(given, 4)
-    paired = (kept.astype(jnp.float32) + from_core.astype(jnp.float32)).astype(jnp.bfloat16)
-    paired = paired.reshape(layers, row_count, half)
-    dealt = deal_rows(layers, paired)
-    total = lax.dynamic_index_in_dim(paired, z, 0, keepdims=False).astype(jnp.float32)
-    for s in range(layers - 1):
-        total = total + dealt[s].astype(jnp.float32)
+    n_fs = layers * PLANE
+
+    def share_of(rows, number):
+        halves = jnp.dot(rows, gu_all, preferred_element_type=jnp.float32)
+        halves = halves.astype(jnp.bfloat16)
+        hidden = (
+            jax.nn.silu(causal_conv(halves[:, :units], gate_taps))
+            * causal_conv(halves[:, units:], value_taps)
+        ).astype(jnp.bfloat16)
+        share = jnp.dot(hidden, dn_all, preferred_element_type=jnp.float32).astype(jnp.bfloat16)
+        kept = lax.dynamic_slice_in_dim(share, tp * half, half, 1)
+        paired = kept.astype(jnp.float32) + swap_halves(share, number).astype(jnp.float32)
+        return paired.astype(jnp.bfloat16)
+
+    def deal(paired, first):
+        sent = []
+        for i in range(paired.shape[0] // row_count):
+            s = first + i
+            block = paired[i * row_count : (i + 1) * row_count]
+            if s == layers:
+                sent.append(block)
+            else:
+                route = [(f, (f + s * PLANE) % n_fs) for f in range(n_fs)]
+                sent.append(lax.ppermute(block, "fs", route))
+        return sent
+
+    cut = layers // 2
+    early_rows, late_rows = normed2[: cut * row_count], normed2[cut * row_count :]
+    early = share_of(early_rows, 4)
+    late_rows, early = lax.optimization_barrier((late_rows, early))
+    dealt = deal(early, 1)
+    late = share_of(late_rows, 5)
+    dealt += deal(late, cut + 1)
+    total = dealt[-1].astype(jnp.float32)
+    for term in dealt[:-1]:
+        total = total + term.astype(jnp.float32)
     residual = lax.dynamic_slice_in_dim(whole_after, tp * half, half, 1)
     return (residual.astype(jnp.float32) + total).astype(jnp.bfloat16)
 

time: 311 us -> 272 us (0.87)
  Pallas kernels: 252 us -> 159 us
  waiting for transfers between devices: 0 us -> 41.2 us
  starting transfers between devices: 0 us -> 6.04 us
    pallas_call x1, Pallas kernels: 138 us -> 91.5 us  [gather_weights(): pl.pallas_call(functools.partial(weights_kernel, layers), out_shape=(shap...]
    pallas_call x2 -> x3, Pallas kernels: 107 us -> 64.8 us  [the longest x1 58.8 us: gather_rows(): pl.pallas_call(functools.partial(rows_kernel, layers), out_shape=(whole,...]
    ppermute x0 -> x3, waiting for transfers between devices: none -> 41.2 us  [deal(): sent.append(lax.ppermute(block, 'fs', route))]
    ppermute x0 -> x3, starting transfers between devices: none -> 6.04 us  [deal(): sent.append(lax.ppermute(block, 'fs', route))]
    pallas_call x2 -> x1, Pallas kernels: 7.54 us -> 3.02 us  [swap_cores(): pl.pallas_call(swap_kernel, out_shape=jax.ShapeDtypeStruct(values.shape,...]
    dot_general x2 -> x4, matrix products: 15.1 us -> 18.4 us  [the longest x2 12.1 us: share_of(): halves = jnp.dot(rows, gu_all, preferred_element_type=jnp.float32)]
    unnamed x34 -> x48, local copies, waits for them, and re-layouts: 4.26 us -> 7.02 us
  transfers between devices with their start and end apart: 0 -> 3, of which waited for: 0 -> 2; matrix products, arithmetic and copies ran while one was open for 0% -> 0% of each run, Pallas kernels for 0% -> 0%
where the time goes in v2:
time: 272 us; the launch traced here: 269 us
  Pallas kernels  159 us (58%)
  waiting for transfers between devices  41.2 us (15%)
  matrix products  24.6 us (9%)
  other arithmetic  21.3 us (8%)
  local copies, waits for them, and re-layouts  15.5 us (6%)
  starting transfers between devices  6.04 us (2%)
    pallas_call x1, Pallas kernels, gather_weights(): pl.pallas_call(functools.partial(weights_kernel, layers), out_shape=(shap...  91.5 us
    pallas_call x1, Pallas kernels, gather_rows(): pl.pallas_call(functools.partial(rows_kernel, layers), out_shape=(whole,...  58.8 us
    ppermute x3, waiting for transfers between devices, deal(): sent.append(lax.ppermute(block, 'fs', route))  41.2 us
    dot_general x2, matrix products, share_of(): halves = jnp.dot(rows, gu_all, preferred_element_type=jnp.float32)  12.1 us
    unnamed x48, local copies, waits for them, and re-layouts  7.02 us
    dot_general x2, matrix products, share_of(): jnp.dot(hidden, dn_all, preferred_element_type=jnp.float32)  6.29 us
    pallas_call x2, Pallas kernels, swap_halves(): pl.pallas_call(swap_half_kernel, out_shape=jax.ShapeDtypeStruct((values.s...  6.04 us
    ppermute x3, starting transfers between devices, deal(): sent.append(lax.ppermute(block, 'fs', route))  6.04 us
  transfers between devices with their start and end apart: 3, of which 2 were waited for; matrix products, arithmetic and copies ran while one was open for 0% of the time, Pallas kernels for 0%

profile of v2, /device:TPU:10, one launch (start us, length us, event | category | flops | bytes accessed | tf_op | source)
XLA Modules:
  0.0 268.9 jit_solution(12277642998273469287)
XLA Ops:
  0.0 1.5 copy.24
  1.5 0.3 copy.26
  1.8 0.3 copy.25
  2.2 0.3 copy.27
  2.5 1.6 maximum_bitcast_fusion.gu
  4.1 0.7 pad_maximum_fusion.bo
  4.8 91.5 %gather_weights.1 = (bf16[256,2048]{1,0:T(8,128)(2,1)}, bf16[2048,1024]{1,0:T(8,128)(2,1)}, bf16[512,2048]{1,0:T(8,128)(2,1)}, bf16[2048,1408]{1,0:T(8,128)(2,1)}, bf16[704,2048]{1,0:T(8,128)(2,1)}) custom-call(bf16[256,1024]{1,0:T(8,128)(2,1)} %tok.1, bf16[128,1024]{1,0:T(8,128)(2,1)} %pad_maximum_fusion.bo, bf16[512,128]{1,0:T(8,128)(2,1)} %mo.1, ...), custom_call_target="tpu_custom_call" | custom-call | tf_op jit(solution)/shard_map/gather_weights/pallas_call | solution.py:300
  96.3 1.5 fusion.3
  97.8 3.8 %convolution_convert_fusion.5 = bf16[256,1024]{1,0:T(8,128)(2,1)S(1)} fusion(bf16[2048,1024]{1,0:T(8,128)(2,1)} %get-tuple-element.16, bf16[256,2048]{1,0:T(8,128)(2,1)} %get-tuple-element.15, f32[2048]{0:T(1024)S(1)} %convert_element_type.227, f32[256]{0:T(256)S(1)} %add_rsqrt_fusion.1), kind=kOutput, calls=%fused_computation.59 | convolution fusion | flops 1076101120 | bytes 5776384 | tf_op jit(solution)/shard_map/dot_general | solution.py:465
  101.8 0.7 copy-done.15
  102.5 0.2 fusion.45
  102.7 0.3 convert_element_type.239
  103.0 0.3 copy.28
  103.3 0.4 fusion.35
  103.7 0.2 copy.30
  103.9 0.3 copy-done.22
  104.2 0.4 fusion.37
  104.6 0.2 copy.33
  104.9 0.4 copy-done.14
  105.3 0.4 fusion.56
  105.7 0.1 slice.256
  105.9 0.1 slice.257
  106.0 0.1 slice.255
  106.2 0.1 slice.259
  107.5 0.2 slice.295
  107.7 0.2 slice.254
  108.7 0.1 pad.66
  109.0 0.3 pad.65
  109.4 1.4 fusion.54
  110.8 1.7 convolution_convert_fusion.4.mine
  112.5 3.0 %swap_cores.1 = bf16[256,2048]{1,0:T(8,128)(2,1)} custom-call(bf16[256,2048]{1,0:T(8,128)(2,1)} %convolution_convert_fusion.4.mine), custom_call_target="tpu_custom_call" | custom-call | tf_op jit(solution)/shard_map/swap_cores/pallas_call | solution.py:331
  115.5 1.9 fusion
  117.4 1.3 fusion.2.mine
  118.7 58.8 %gather_rows.1 = (bf16[1024,2048]{1,0:T(8,128)(2,1)}, bf16[2048,1408]{1,0:T(8,128)(2,1)}, bf16[704,2048]{1,0:T(8,128)(2,1)}) custom-call(bf16[256,2048]{1,0:T(8,128)(2,1)} %fusion.2.mine, bf16[2048,1408]{1,0:T(8,128)(2,1)} %get-tuple-element.18.gu_in, bf16[704,2048]{1,0:T(8,128)(2,1)} %get-tuple-element.19.dn_in), custom_call_target="tpu_custom_call", output_to_operand_aliasing={{1}: (1, {}), {2}: (2, {})} | custom-call | tf_op jit(solution)/shard_map/gather_rows/pallas_call | solution.py:384
  177.5 3.3 %slice.297 = bf16[512,2048]{1,0:T(8,128)(2,1)} slice(bf16[1024,2048]{1,0:T(8,128)(2,1)} %get-tuple-element.20), slice={[512:1024], [0:2048]} | slice | bytes 4194304 | tf_op jit(solution)/shard_map/slice | solution.py:522
  180.9 6.1 %convolution_convert_fusion.3 = bf16[512,1408]{1,0:T(8,128)(2,1)S(1)} fusion(bf16[2048,1408]{1,0:T(8,128)(2,1)} %get-tuple-element.21, bf16[1024,2048]{1,0:T(8,128)(2,1)S(1)} %copy-done.12), kind=kOutput, calls=%fused_computation.6 | convolution fusion | flops 2953510912 | bytes 9306112 | tf_op jit(solution)/shard_map/dot_general | solution.py:498
  186.9 0.5 fusion.71
  187.4 0.1 convert.17
  187.5 1.3 convert.18
  188.9 0.9 fusion.65
  189.8 0.5 fusion.10
  190.3 0.9 copy-done.3
  191.2 0.5 fusion.14
  191.7 0.5 fusion.28
  192.2 1.3 copy-done.8
  193.5 3.1 %convolution_convert_fusion.2.mine = bf16[512,2048]{1,0:T(8,128)(2,1)} fusion(bf16[512,704]{1,0:T(8,128)(2,1)S(1)} %fusion.28, bf16[704,2048]{1,0:T(8,128)(2,1)S(1)} %copy-done.8), kind=kOutput, calls=%fused_computation.5 | convolution fusion | flops 1477443584 | bytes 5701632 | tf_op jit(solution)/shard_map/dot_general | solution.py:504
  196.6 3.0 %swap_halves.2 = bf16[512,1024]{1,0:T(8,128)(2,1)} custom-call(bf16[512,2048]{1,0:T(8,128)(2,1)} %convolution_convert_fusion.2.mine), custom_call_target="tpu_custom_call" | custom-call | tf_op jit(solution)/shard_map/swap_halves/pallas_call | solution.py:416
  199.7 2.8 %add_convert_fusion.1 = bf16[512,1024]{1,0:T(8,128)(2,1)} fusion(bf16[512,1024]{1,0:T(8,128)(2,1)} %swap_halves.2, bf16[512,2048]{1,0:T(8,128)(2,1)S(1)} %copy-done.4, s32[]{:T(128)S(6)} %select_n.14), kind=kLoop, calls=%fused_computation.18 | loop fusion | flops 2097152 | bytes 3145732 | tf_op jit(solution)/shard_map/convert_element_type | solution.py:507
  202.5 6.1 %convolution_convert_fusion.1 = bf16[512,1408]{1,0:T(8,128)(2,1)S(1)} fusion(bf16[512,2048]{1,0:T(8,128)(2,1)S(1)} %copy-done.10, bf16[2048,1408]{1,0:T(8,128)(2,1)} %get-tuple-element.21), kind=kOutput, calls=%fused_computation.4 | convolution fusion | flops 2953510912 | bytes 9306112 | tf_op jit(solution)/shard_map/dot_general | solution.py:498
  208.5 0.5 fusion.70
  209.0 0.1 convert.19
  209.2 0.5 fusion.18
  209.6 0.1 convert.20
  209.8 0.7 fusion.22
  210.5 0.5 fusion.24
  211.0 1.3 copy-done.9
  212.3 3.2 %convolution_convert_fusion.mine = bf16[512,2048]{1,0:T(8,128)(2,1)} fusion(bf16[512,704]{1,0:T(8,128)(2,1)S(1)} %fusion.24, bf16[704,2048]{1,0:T(8,128)(2,1)S(1)} %copy-done.9), kind=kOutput, calls=%fused_computation.3 | convolution fusion | flops 1477443584 | bytes 5701632 | tf_op jit(solution)/shard_map/dot_general | solution.py:504
  215.5 3.0 %swap_halves.3 = bf16[512,1024]{1,0:T(8,128)(2,1)} custom-call(bf16[512,2048]{1,0:T(8,128)(2,1)} %convolution_convert_fusion.mine), custom_call_target="tpu_custom_call" | custom-call | tf_op jit(solution)/shard_map/swap_halves/pallas_call | solution.py:416
  218.5 1.7 add_convert_fusion
  220.4 2.1 collective-permute-start
  222.5 3.9 %collective-permute-start.1 = (bf16[256,1024]{1,0:T(8,128)(2,1)S(1)}, bf16[256,1024]{1,0:T(8,128)(2,1)S(1)}, u32[]{:S(2)}, u32[]{:S(2)}) collective-permute-start(bf16[256,1024]{1,0:T(8,128)(2,1)S(1)} %get-tuple-element.40), channel_id=1, source_target_pairs={{0,16},{2,18},{4,20},{6,22},{8,24},{10,26},{12,28},{14,30},{16,0},... | collective-permute-start | bytes 1572872 | tf_op jit(solution)/shard_map/ppermute | solution.py:518
  226.4 31.2 %collective-permute-done.2 = bf16[256,1024]{1,0:T(8,128)(2,1)S(1)} collective-permute-done((bf16[256,1024]{1,0:T(8,128)(2,1)S(1)}, bf16[256,1024]{1,0:T(8,128)(2,1)S(1)}, u32[]{:S(2)}, u32[]{:S(2)}) %collective-permute-start.2) | collective-permute-done | bytes 524320 | tf_op jit(solution)/shard_map/ppermute | solution.py:518
  257.6 10.0 %collective-permute-done.1 = bf16[256,1024]{1,0:T(8,128)(2,1)S(1)} collective-permute-done((bf16[256,1024]{1,0:T(8,128)(2,1)S(1)}, bf16[256,1024]{1,0:T(8,128)(2,1)S(1)}, u32[]{:S(2)}, u32[]{:S(2)}) %collective-permute-start.1) | collective-permute-done | bytes 524320 | tf_op jit(solution)/shard_map/ppermute | solution.py:518
  267.6 1.3 add_convert_fusion.2
  (108 shorter events, 2.4 us)
Async XLA Ops:
  0.0 103.3 %copy-start = (bf16[8,64,64]{2,1,0:T(8,128)(2,1)S(1)}, bf16[8,64,64]{2,1,0:T(8,128)(2,1)}, u32[]{:S(2)}) copy-start(bf16[8,64,64]{2,1,0:T(8,128)(2,1)} %param.21) | copy-start | bytes 196612
  0.0 1.8 copy-start.13
  2.5 1.6 copy-start.16
  2.5 1.6 copy-start.17
  4.8 93.0 %copy-start.19 = (bf16[2048]{0:T(1024)(128)(2,1)S(1)}, bf16[2048]{0:T(1024)(128)(2,1)}, u32[]{:S(2)}) copy-start(bf16[2048]{0:T(1024)(128)(2,1)} %param.17) | copy-start | bytes 12292
  97.8 3.9 %copy-start.18 = (bf16[4,512]{1,0:T(4,128)(2,1)S(1)}, bf16[4,512]{1,0:T(4,128)(2,1)}, u32[]{:S(2)}) copy-start(bf16[4,512]{1,0:T(4,128)(2,1)} %param.20) | copy-start | bytes 12292
  101.7 0.8 copy-start.15
  103.3 0.9 copy-start.22
  104.2 0.7 copy-start.21
  104.2 1.1 copy-start.14
  109.0 1.8 copy-start.11
  112.5 3.0 %copy-start.2 = (bf16[256,2048]{1,0:T(8,128)(2,1)S(1)}, bf16[256,2048]{1,0:T(8,128)(2,1)}, u32[]{:S(2)}) copy-start(bf16[256,2048]{1,0:T(8,128)(2,1)} %convolution_convert_fusion.4.mine) | copy-start | bytes 3145732
  112.5 3.0 %copy-start.6 = (bf16[256,2048]{1,0:T(8,128)(2,1)S(1)}, bf16[256,2048]{1,0:T(8,128)(2,1)}, u32[]{:S(2)}) copy-start(bf16[256,2048]{1,0:T(8,128)(2,1)} %get-tuple-element.15) | copy-start | bytes 3145732
  115.5 1.9 copy-start.20
  177.5 3.3 %copy-start.12 = (bf16[1024,2048]{1,0:T(8,128)(2,1)S(1)}, bf16[1024,2048]{1,0:T(8,128)(2,1)}, u32[]{:S(2)}) copy-start(bf16[1024,2048]{1,0:T(8,128)(2,1)} %get-tuple-element.20) | copy-start | bytes 12582916
  189.8 1.4 copy-start.3
  191.7 1.8 copy-start.8
  196.6 3.0 %copy-start.4 = (bf16[512,2048]{1,0:T(8,128)(2,1)S(1)}, bf16[512,2048]{1,0:T(8,128)(2,1)}, u32[]{:S(2)}) copy-start(bf16[512,2048]{1,0:T(8,128)(2,1)} %convolution_convert_fusion.2.mine) | copy-start | bytes 6291460
  199.7 2.8 %copy-start.10 = (bf16[512,2048]{1,0:T(8,128)(2,1)S(1)}, bf16[512,2048]{1,0:T(8,128)(2,1)}, u32[]{:S(2)}) copy-start(bf16[512,2048]{1,0:T(8,128)(2,1)} %slice.297) | copy-start | bytes 6291460
  210.5 1.8 copy-start.9
  215.5 3.0 %copy-start.5 = (bf16[512,2048]{1,0:T(8,128)(2,1)S(1)}, bf16[512,2048]{1,0:T(8,128)(2,1)}, u32[]{:S(2)}) copy-start(bf16[512,2048]{1,0:T(8,128)(2,1)} %convolution_convert_fusion.mine) | copy-start | bytes 6291460
  218.5 1.8 copy-start.7
  220.3 37.3 %collective-permute-start.2 = (bf16[256,1024]{1,0:T(8,128)(2,1)S(1)}, bf16[256,1024]{1,0:T(8,128)(2,1)S(1)}, u32[]{:S(2)}, u32[]{:S(2)}) collective-permute-start(bf16[256,1024]{1,0:T(8,128)(2,1)S(1)} %slice.349), channel_id=1, source_target_pairs={{0,24},{2,26},{4,28},{6,30},{8,0},{10,2},{12,4},{14,6},{16,8},{18,... | collective-permute-start | bytes 1572872 | tf_op jit(solution)/shard_map/ppermute | solution.py:518
  220.4 37.2 %collective-permute-start = (bf16[256,1024]{1,0:T(8,128)(2,1)S(1)}, bf16[256,1024]{1,0:T(8,128)(2,1)S(1)}, u32[]{:S(2)}, u32[]{:S(2)}) collective-permute-start(bf16[256,1024]{1,0:T(8,128)(2,1)S(1)} %get-tuple-element.39), channel_id=1, source_target_pairs={{0,8},{2,10},{4,12},{6,14},{8,16},{10,18},{12,20},{14,22},{16,24},... | collective-permute-start | bytes 1572872 | tf_op jit(solution)/shard_map/ppermute | solution.py:518
  222.5 46.4 %copy-start.1 = (bf16[8,64,64]{2,1,0:T(8,128)(2,1)S(1)}, bf16[8,64,64]{2,1,0:T(8,128)(2,1)}, u32[]{:S(2)}) copy-start(bf16[8,64,64]{2,1,0:T(8,128)(2,1)} %param.21) | copy-start | bytes 196612
  222.5 45.1 %collective-permute-start.1 = (bf16[256,1024]{1,0:T(8,128)(2,1)S(1)}, bf16[256,1024]{1,0:T(8,128)(2,1)S(1)}, u32[]{:S(2)}, u32[]{:S(2)}) collective-permute-start(bf16[256,1024]{1,0:T(8,128)(2,1)S(1)} %get-tuple-element.40), channel_id=1, source_target_pairs={{0,16},{2,18},{4,20},{6,22},{8,24},{10,26},{12,28},{14,30},{16,0},... | collective-permute-start | bytes 1572872 | tf_op jit(solution)/shard_map/ppermute | solution.py:518
